TPU v7x, 32 devices: a whole 2x2x4 slice. The times are simulated.
32 devices in a mesh: fs: 8 (over z, y), tp: 4 (over x, core).
Axes of the slice: x: 2, y: 2, z: 4, core: 2. Of those that a mesh axis runs over, the one named last changes fastest.
Arguments:
- late_input: bfloat16 [2048, 2048], P(('fs', 'tp')), may hold values from -6 to 6
- early_input: bfloat16 [2048, 2048], P(('fs', 'tp')), may hold values from -6 to 6
- early_grad: bfloat16 [2048, 2048], P(('fs', 'tp')), may hold values from -6 to 6
- pre_gain: float32 [2048], replicated, may hold values from 0.1 to 1.9
- post_gain: float32 [2048], replicated, may hold values from 0.1 to 1.9
- gate_weight: bfloat16 [2048, 4096], P('fs', 'tp'), may hold values from -0.125 to 0.125
- up_weight: bfloat16 [2048, 4096], P('fs', 'tp'), may hold values from -0.125 to 0.125
- down_weight: bfloat16 [2048, 4096], P('fs', 'tp'), may hold values from -0.09375 to 0.09375
- gate_sum: float32 [2048, 4096], P('fs', 'tp'), may hold values from -1.8 to 1.8
- up_sum: float32 [2048, 4096], P('fs', 'tp'), may hold values from -1.8 to 1.8
- down_gradient_sum: float32 [2048, 4096], P('fs', 'tp'), may hold values from -1.8 to 1.8
Outputs:
- late_output: bfloat16 [2048, 2048], P(('fs', 'tp'))
- early_input_grad: bfloat16 [2048, 2048], P(('fs', 'tp'))
- gate_total: float32 [2048, 4096], P('fs', 'tp')
- up_total: float32 [2048, 4096], P('fs', 'tp')
- down_total: float32 [2048, 4096], P('fs', 'tp')
All inputs are finite; a program needn't handle non-finite values.
Results may differ from a plain program's by a relative error of at most 0.013.
Values may be sent and summed in bfloat16 or wider, within the bound.
A program may use at most 128 MiB of HBM per device.

v0:
```python
import math

import jax
import jax.numpy as jnp
from jax import lax
from jax.sharding import PartitionSpec as P

NORM_EPS = 1e-06


def contract_last(first_op, second_op):
    return lax.dot_general(
        first_op, second_op, (((1,), (1,)), ((), ())), preferred_element_type=jnp.float32
    )


def contract_first(first_op, second_op):
    return lax.dot_general(
        first_op, second_op, (((0,), (0,)), ((), ())), preferred_element_type=jnp.float32
    )


def inverse_rms(values):
    return lax.rsqrt(jnp.mean(values * values, axis=-1, keepdims=True) + NORM_EPS)


def per_device(
    late_input,
    early_input,
    early_grad,
    pre_gain,
    post_gain,
    gate_weight,
    up_weight,
    down_weight,
    gate_sum,
    up_sum,
    down_gradient_sum,
):
    tok_rows, model_width = late_input.shape
    group_rows = tok_rows * lax.axis_size("tp")
    grad_scale = 1.0 / math.sqrt(group_rows * lax.axis_size("fs"))
    hidden_width = gate_sum.shape[1]
    input_rows = jnp.stack([late_input, early_input]).astype(jnp.float32)
    input_inverse = inverse_rms(input_rows)
    normed = (input_rows * input_inverse * pre_gain).astype(jnp.bfloat16)
    normed_rows = lax.all_gather(normed, "tp", axis=1, tiled=True)
    gate_all, up_all, down_gradient_rows = (
        lax.all_gather(gate_weight, "fs", axis=0, tiled=True),
        lax.all_gather(up_weight, "fs", axis=0, tiled=True),
        lax.all_gather(down_weight, "fs", axis=0, tiled=True),
    )
    flat_rows = normed_rows.reshape(2 * group_rows, model_width)
    gate_pre = jnp.dot(flat_rows, gate_all, preferred_element_type=jnp.float32)
    up_pre = jnp.dot(flat_rows, up_all, preferred_element_type=jnp.float32)
    hidden_state = (
        (jax.nn.silu(gate_pre) * up_pre).astype(jnp.bfloat16).reshape(2, group_rows, hidden_width)
    )
    gated_product = jnp.einsum(
        "utx,ix->tui", hidden_state, down_gradient_rows, preferred_element_type=jnp.float32
    )
    mixed_sum = lax.psum_scatter(
        gated_product.reshape(lax.axis_size("tp") * tok_rows, 2 * model_width).astype(jnp.bfloat16),
        "tp",
        scatter_dimension=0,
        tiled=True,
    ).astype(jnp.float32)
    mixed_sum = lax.optimization_barrier(mixed_sum.astype(jnp.bfloat16)).astype(jnp.float32)
    mixed_sum = mixed_sum.reshape(tok_rows, 2, model_width)
    mixed_inverse = inverse_rms(mixed_sum)
    late_output = (input_rows[0] + 0.5 * mixed_sum[:, 0] * mixed_inverse[:, 0] * post_gain).astype(
        jnp.bfloat16
    )
    early_mixed = mixed_sum[:, 1]
    early_inverse_norm = mixed_inverse[:, 1]
    weighted = 0.5 * early_grad.astype(jnp.float32) * post_gain
    mixed_cot = (
        early_inverse_norm * weighted
        - early_mixed
        * early_inverse_norm**3
        * jnp.mean(weighted * early_mixed, axis=-1, keepdims=True)
    ).astype(jnp.bfloat16)
    cot_rows = lax.all_gather(mixed_cot, "tp", axis=0, tiled=True)
    early_hidden = hidden_state[1]
    early_normed = normed_rows[1]
    hidden_cot = jnp.dot(cot_rows, down_gradient_rows, preferred_element_type=jnp.float32)
    early_gate = gate_pre[group_rows:]
    early_up = up_pre[group_rows:]
    sigmoid_gate = jax.nn.sigmoid(early_gate)
    gate_cot = (
        hidden_cot * early_up * sigmoid_gate * (1.0 + early_gate * (1.0 - sigmoid_gate))
    ).astype(jnp.bfloat16)
    up_cot = (hidden_cot * early_gate * sigmoid_gate).astype(jnp.bfloat16)
    normed_cot = lax.psum_scatter(
        (contract_last(gate_cot, gate_all) + contract_last(up_cot, up_all)).astype(jnp.bfloat16),
        "tp",
        scatter_dimension=0,
        tiled=True,
    ).astype(jnp.float32)
    normed_cot = lax.optimization_barrier(normed_cot.astype(jnp.bfloat16)).astype(jnp.float32)
    weighted_in = normed_cot * pre_gain
    early_values = input_rows[1]
    early_in_inverse = input_inverse[1]
    early_input_grad = (
        early_grad.astype(jnp.float32)
        + early_in_inverse * weighted_in
        - early_values
        * early_in_inverse**3
        * jnp.mean(weighted_in * early_values, axis=-1, keepdims=True)
    ).astype(jnp.bfloat16)
    totals = lax.psum_scatter(
        (
            grad_scale
            * jnp.concatenate(
                [
                    contract_first(early_normed, gate_cot),
                    contract_first(early_normed, up_cot),
                    contract_first(cot_rows, early_hidden),
                ],
                1,
            )
        ).astype(jnp.bfloat16),
        "fs",
        scatter_dimension=0,
        tiled=True,
    ).astype(jnp.float32)
    gate_total = gate_sum + totals[:, :hidden_width]
    up_total = up_sum + totals[:, hidden_width : 2 * hidden_width]
    down_total = down_gradient_sum + totals[:, 2 * hidden_width :]
    return (late_output, early_input_grad, gate_total, up_total, down_total)


def solution(mesh):
    in_specs = (
        P(("fs", "tp"), None),
        P(("fs", "tp"), None),
        P(("fs", "tp"), None),
        P(),
        P(),
        P("fs", "tp"),
        P("fs", "tp"),
        P("fs", "tp"),
        P("fs", "tp"),
        P("fs", "tp"),
        P("fs", "tp"),
    )
    out_specs = (
        P(("fs", "tp"), None),
        P(("fs", "tp"), None),
        P("fs", "tp"),
        P("fs", "tp"),
        P("fs", "tp"),
    )
    return jax.shard_map(
        per_device, mesh=mesh, in_specs=in_specs, out_specs=out_specs, check_vma=False
    )
```

profile of v0, /device:TPU:16, one launch (start us, length us, event | category | flops | bytes accessed | tf_op | source)
XLA Modules:
  0.0 582.8 jit_solution(17200032101775942609)
XLA Ops:
  7.2 1.2 multiply_reduce_fusion.1
  8.4 2.0 multiply_convert_fusion.2
  10.5 0.7 all-gather.8.cloned.1.call-update
  11.3 0.7 all-gather.10.cloned.1.call-update
  12.0 0.5 all-gather.12.cloned.1.call-update
  12.6 21.7 %all-gather.6.cloned.1.call-done = bf16[2,256,2048]{2,1,0:T(8,128)(2,1)} async-done(((bf16[2,64,2048]{2,1,0:T(8,128)(2,1)}), bf16[2,256,2048]{2,1,0:T(8,128)(2,1)}) %all-gather.6.cloned.1.call-update) | async-done | bytes 2097168 | tf_op jit(solution)/shard_map/all_gather | solution.py:47
  34.3 74.4 %all-gather.8.cloned.1.call-done = bf16[2048,1024]{1,0:T(8,128)(2,1)} async-done(((bf16[256,1024]{1,0:T(8,128)(2,1)}), bf16[2048,1024]{1,0:T(8,128)(2,1)}) %all-gather.8.cloned.1.call-update) | async-done | bytes 4194320 | tf_op jit(solution)/shard_map/all_gather | solution.py:49
  108.7 6.6 %fusion.29 = f32[512,1024]{1,0:T(8,128)} fusion(bf16[512,2048]{1,0:T(8,128)(2,1)} %bitcast.71, bf16[2048,1024]{1,0:T(8,128)(2,1)} %all-gather.8.cloned.1.call-done), kind=kOutput, calls=%fused_computation.57 | convolution fusion | flops 2147483648 | bytes 8388608 | tf_op jit(solution)/shard_map/dot_general | solution.py:54
  115.3 66.9 %all-gather.10.cloned.1.call-done = bf16[2048,1024]{1,0:T(8,128)(2,1)} async-done(((bf16[256,1024]{1,0:T(8,128)(2,1)}), bf16[2048,1024]{1,0:T(8,128)(2,1)}) %all-gather.10.cloned.1.call-update) | async-done | bytes 4194320 | tf_op jit(solution)/shard_map/all_gather | solution.py:50
  182.2 6.6 %multiply_convert_fusion = (bf16[512,1024]{1,0:T(8,128)(2,1)S(1)}, f32[512,1024]{1,0:T(8,128)}) fusion(f32[512,1024]{1,0:T(8,128)} %fusion.29, bf16[512,2048]{1,0:T(8,128)(2,1)S(1)} %bitcast.72, bf16[2048,1024]{1,0:T(8,128)(2,1)} %all-gather.10.cloned.1.call-done), kind=kOutput, calls=%fused_computation.8 | convolution fusion | flops 2150629376 | bytes 11534336 | tf_op jit(solution)/shard_map/dot_general | solution.py:55
  188.8 66.8 %all-gather.12.cloned.1.call-done = bf16[2048,1024]{1,0:T(8,128)(2,1)} async-done(((bf16[256,1024]{1,0:T(8,128)(2,1)}), bf16[2048,1024]{1,0:T(8,128)(2,1)}) %all-gather.12.cloned.1.call-update) | async-done | bytes 4194320 | tf_op jit(solution)/shard_map/all_gather | solution.py:51
  255.5 5.9 %fusion.6 = bf16[256,2,2048]{2,0,1:T(8,128)(2,1)} fusion(bf16[2,256,1024]{2,1,0:T(8,128)(2,1)S(1)} %bitcast.79, bf16[2048,1024]{1,0:T(8,128)(2,1)} %all-gather.12.cloned.1.call-done), kind=kOutput, calls=%fused_computation.5 | convolution fusion | flops 2148532224 | bytes 7340032 | tf_op jit(solution)/shard_map/utx,ix->tui/dot_general | solution.py:59
  261.4 2.8 copy.43
  264.2 2.9 copy.54
  267.2 0.0 all-gather.14.cloned.1.call-start
  267.3 30.3 %reduce-scatter.10.cloned.1.call-done = bf16[64,4096]{1,0:T(8,128)(2,1)} async-done(((bf16[256,4096]{1,0:T(8,128)(2,1)}), bf16[64,4096]{1,0:T(8,128)(2,1)}) %reduce-scatter.10.cloned.1.call-update) | async-done | bytes 524304
  297.6 1.5 copy.55
  299.1 0.3 copy.44
  299.5 1.0 reshape.119
  300.5 1.6 fusion.28
  302.1 0.5 multiply_reduce_fusion
  302.6 0.1 copy.58
  302.7 0.3 fusion.19
  303.0 1.0 fusion.18
  304.0 0.2 reduce-scatter.6.cloned.1.call-start
  304.2 16.6 %all-gather.14.cloned.1.call-done = bf16[256,2048]{1,0:T(8,128)(2,1)} async-done(((bf16[64,2048]{1,0:T(8,128)(2,1)}), bf16[256,2048]{1,0:T(8,128)(2,1)}) %all-gather.14.cloned.1.call-update) | async-done | bytes 1048592 | tf_op jit(solution)/shard_map/all_gather | solution.py:83
  320.8 4.7 multiply_convert_fusion.1
  325.6 1.3 fusion.30
  326.9 1.2 copy-done.16
  328.2 2.3 fusion.9
  330.5 2.5 fusion.22
  333.1 1.3 fusion.13
  334.4 1.3 fusion.14
  335.7 7.5 %fusion = bf16[2048,3072]{0,1:T(8,128)(2,1)} fusion(f32[2048,1024]{0,1:T(8,128)S(1)} %fusion.22, f32[2048,1024]{0,1:T(8,128)S(1)} %fusion.13, f32[2048,1024]{0,1:T(8,128)S(1)} %fusion.14), kind=kLoop, calls=%fused_computation.1 | loop fusion | flops 25165824 | bytes 37748736 | tf_op jit(solution)/shard_map/convert_element_type | solution.py:122
  343.2 1.2 copy-done.6
  344.4 0.3 copy.50
  344.8 0.3 copy.49
  345.1 2.5 copy.48
  347.7 1.1 maximum_convert_fusion
  348.8 6.6 %reduce-scatter.6.cloned.1.call-done = bf16[64,2048]{1,0:T(8,128)(2,1)} async-done(((bf16[256,2048]{1,0:T(8,128)(2,1)}), bf16[64,2048]{1,0:T(8,128)(2,1)}) %reduce-scatter.6.cloned.1.call-update) | async-done | bytes 262160 | tf_op jit(solution)/shard_map/reduce_scatter | solution.py:94
  355.4 1.1 multiply_reduce_fusion.2
  356.5 2.2 fusion.21
  358.8 207.2 %reduce-scatter.8.cloned.1.call-done = bf16[256,3072]{0,1:T(8,128)(2,1)} async-done(((bf16[2048,3072]{0,1:T(8,128)(2,1)}), bf16[256,3072]{0,1:T(8,128)(2,1)}) %reduce-scatter.8.cloned.1.call-update) | async-done | bytes 1572880 | tf_op jit(solution)/shard_map/reduce_scatter | solution.py:111
  566.0 1.6 convert_element_type.69
  567.7 1.8 slice_add_fusion
  569.5 2.6 copy.51
  572.1 2.5 copy.52
  574.6 1.3 copy.53
  (51 shorter events, 0.4 us)
Async XLA Ops:
  7.2 27.1 %all-gather.6.cloned.1.call-start = ((), (), s32[]{:S(2)}) async-start(), calls=%async_computation.3 | async-start | bytes 2621440 | tf_op jit(solution)/shard_map/all_gather | solution.py:47
  10.5 98.2 %all-gather.8.cloned.1.call-start = ((), (), s32[]{:S(2)}) async-start(), calls=%async_computation.4 | async-start | bytes 4718592 | tf_op jit(solution)/shard_map/all_gather | solution.py:49
  11.2 170.9 %all-gather.10.cloned.1.call-start = ((), (), s32[]{:S(2)}) async-start(), calls=%async_computation.5 | async-start | bytes 4718592 | tf_op jit(solution)/shard_map/all_gather | solution.py:50
  12.0 243.5 %all-gather.12.cloned.1.call-start = ((), (), s32[]{:S(2)}) async-start(), calls=%async_computation.6 | async-start | bytes 4718592 | tf_op jit(solution)/shard_map/all_gather | solution.py:51
  12.6 285.0 %reduce-scatter.10.cloned.1.call-start = ((), (), s32[]{:S(2)}) async-start(), calls=%async_computation.10 | async-start | bytes 2621440
  108.7 73.5 %copy-start.2 = (bf16[2,256,2048]{2,1,0:T(8,128)(2,1)S(1)}, bf16[2,256,2048]{2,1,0:T(8,128)(2,1)}, u32[]{:S(2)}) copy-start(bf16[2,256,2048]{2,1,0:T(8,128)(2,1)} %all-gather.6.cloned.1.call-done) | copy-start | bytes 6291460
  188.7 72.6 %copy-start.12 = (bf16[512,1024]{1,0:T(8,128)(2,1)}, bf16[512,1024]{1,0:T(8,128)(2,1)S(1)}, u32[]{:S(2)}) copy-start(bf16[512,1024]{1,0:T(8,128)(2,1)S(1)} %get-tuple-element.36) | copy-start | bytes 3145732
  264.2 3.0 copy-start.14
  267.2 35.5 %copy-start.4 = (bf16[64,2048]{1,0:T(8,128)(2,1)S(1)}, bf16[64,2048]{1,0:T(8,128)(2,1)}, u32[]{:S(2)}) copy-start(bf16[64,2048]{1,0:T(8,128)(2,1)} %param.13) | copy-start | bytes 786436
  267.2 53.6 %all-gather.14.cloned.1.call-start = ((), (), s32[]{:S(2)}) async-start(), calls=%async_computation.7 | async-start | bytes 1310720 | tf_op jit(solution)/shard_map/all_gather | solution.py:83
  304.0 51.4 %reduce-scatter.6.cloned.1.call-start = ((), (), s32[]{:S(2)}) async-start(), calls=%async_computation.8 | async-start | bytes 1310720 | tf_op jit(solution)/shard_map/reduce_scatter | solution.py:94
  320.8 4.8 copy-start.15
  325.6 1.3 copy-start.8
  325.6 4.8 copy-start.10
  325.6 2.6 copy-start.16
  328.2 2.4 copy-start.5
  330.5 2.6 copy-start.3
  330.5 235.5 %reduce-scatter.8.cloned.1.call-start = ((), (), s32[]{:S(2)}) async-start(), calls=%async_computation.9 | async-start | bytes 14155776 | tf_op jit(solution)/shard_map/reduce_scatter | solution.py:111
  330.5 2.5 copy-start.11
  333.0 1.3 copy-start.9
  343.2 1.2 copy-start.6
  343.2 1.6 copy-start.7
  344.4 11.0 %copy-start.13 = (f32[2048]{0:T(1024)S(1)}, f32[2048]{0:T(1024)}, u32[]{:S(2)}) copy-start(f32[2048]{0:T(1024)} %param.14) | copy-start | bytes 24580
  358.8 208.9 %copy-start = (f32[256,1024]{0,1:T(8,128)S(1)}, f32[256,1024]{0,1:T(8,128)}, u32[]{:S(2)}) copy-start(f32[256,1024]{0,1:T(8,128)} %copy.48) | copy-start | bytes 3145732
  569.5 5.2 copy-start.1
Sparse Core Ops, SparseCore 0:
  10.6 23.6 all-gather.5
  36.4 72.2 all-gather.7
  110.8 71.3 all-gather.9
  184.2 71.3 all-gather.11
  267.3 30.2 reduce-scatter.9
  304.1 16.6 all-gather.13
  330.6 24.7 reduce-scatter.5
  359.0 206.9 reduce-scatter.7
where the time goes:
time: 586 us; the launch traced here: 583 us
  waiting for transfers between devices  492 us (84%)
  matrix products  32.4 us (6%)
  local copies, waits for them, and re-layouts  22.5 us (4%)
  other arithmetic  20.5 us (3%)
  between operations  14.4 us (2%)
    reduce_scatter x1, waiting for transfers between devices, per_device(): lax.psum_scatter((grad_scale * jnp.concatenate([contract_first(early_norm...  207 us
    all_gather x1, waiting for transfers between devices, per_device(): lax.all_gather(gate_weight, 'fs', axis=0, tiled=True)  74.4 us
    all_gather x1, waiting for transfers between devices, per_device(): lax.all_gather(up_weight, 'fs', axis=0, tiled=True)  66.9 us
    all_gather x1, waiting for transfers between devices, per_device(): lax.all_gather(down_weight, 'fs', axis=0, tiled=True)  66.8 us
    unnamed x9, waiting for transfers between devices  32.3 us
    all_gather x1, waiting for transfers between devices, per_device(): normed_rows = lax.all_gather(normed, 'tp', axis=1, tiled=True)  21.7 us
    unnamed x43, local copies, waits for them, and re-layouts  16.7 us
    all_gather x1, waiting for transfers between devices, per_device(): cot_rows = lax.all_gather(mixed_cot, 'tp', axis=0, tiled=True)  16.6 us
  transfers between devices with their start and end apart: 8, of which 8 were waited for; matrix products, arithmetic and copies ran while one was open for 6% of the time, Pallas kernels for 0%

commit v1 on v0

v1 whole, which is shorter than its diff:
```python
import functools
import math

import jax
import jax.numpy as jnp
from jax import lax
from jax.experimental import pallas as pl
from jax.experimental.pallas import tpu as pltpu
from jax.sharding import PartitionSpec as P

NORM_EPS = 1e-06
PAIR = 2
MESH = pl.DeviceIdType.MESH
VMEM_LIMIT = 60 * 1024 * 1024


def contract_last(first_op, second_op):
    return lax.dot_general(
        first_op, second_op, (((1,), (1,)), ((), ())), preferred_element_type=jnp.float32
    )


def contract_first(first_op, second_op):
    return lax.dot_general(
        first_op, second_op, (((0,), (0,)), ((), ())), preferred_element_type=jnp.float32
    )


def inverse_rms(values):
    return lax.rsqrt(jnp.mean(values * values, axis=-1, keepdims=True) + NORM_EPS)


class Place:
    def __init__(self, n_fs, n_tp):
        self.line_len, self.n_tp = n_fs // PAIR, n_tp
        self.group = PAIR * n_tp
        self.fs, self.tp = lax.axis_index("fs"), lax.axis_index("tp")
        self.line, self.side = self.fs // PAIR, self.fs % PAIR
        self.member = self.side * n_tp + self.tp
        self.core = self.tp % PAIR
        self.chip = self.member // PAIR
        self.up = {"fs": self.fs + PAIR, "tp": self.tp}
        self.down = {"fs": self.fs - PAIR, "tp": self.tp}
        self.across = {"fs": self.line * PAIR + 1 - self.side, "tp": self.tp}
        self.has_up, self.has_down = self.line < self.line_len - 1, self.line > 0

    def member_id(self, member):
        return {"fs": self.line * PAIR + member // self.n_tp, "tp": member % self.n_tp}

    def enter(self, on_line):
        barrier = pltpu.get_barrier_semaphore()

        def greet(who):
            pl.semaphore_signal(barrier, inc=1, device_id=who, device_id_type=MESH)

        for offset in range(1, self.group):
            greet(self.member_id((self.member + offset) % self.group))
        if on_line:
            pl.when(self.has_up)(lambda: greet(self.up))
            pl.when(self.has_down)(lambda: greet(self.down))
        peers = self.group - 1
        if on_line:
            peers += self.has_up.astype(jnp.int32) + self.has_down.astype(jnp.int32)
        pl.semaphore_wait(barrier, peers)


def remote(src, dst, send_sem, recv_sem, who):
    return pltpu.make_async_remote_copy(
        src_ref=src,
        dst_ref=dst,
        send_sem=send_sem,
        recv_sem=recv_sem,
        device_id=who,
        device_id_type=MESH,
    )


def gather_kernel(
    n_fs,
    n_tp,
    late_ref,
    early_ref,
    *refs,
):
    w_refs, (late_out, early_out), w_outs = refs[:3], refs[3:5], refs[5:8]
    tok_send, tok_recv, own_sem, across_send, up_send, down_send, w_recv = refs[8:]
    at = Place(n_fs, n_tp)
    half = w_outs[0].shape[2]
    kept = pl.ds(pl.multiple_of(at.side * half, half), half)
    given = pl.ds(pl.multiple_of((1 - at.side) * half, half), half)
    at.enter(True)

    def slot_of(line, turn):
        return line * PAIR + (at.side if turn == 0 else 1 - at.side)

    def carry(w, slot, src, send_sem, who):
        return remote(src, w_outs[w].at[slot], send_sem, w_recv.at[w, slot], who)

    across, own, tokens = [], [], []
    for w in range(3):
        across.append(
            carry(w, at.fs, w_refs[w].at[:, given], across_send.at[w], at.across)
        )
        across[-1].start()
    flows = []
    for step in range(at.line_len):
        for w in range(3):
            for turn in range(PAIR):
                from_low, from_high = at.line - step, at.line + step
                low = jnp.maximum(from_low, 0)
                high = jnp.minimum(from_high, at.line_len - 1)
                flows.append((step, w, turn, from_low >= 0, from_high < at.line_len, low, high))

    def flow_copies(flow):
        step, w, turn, _, _, low, high = flow
        own_block = step == 0 and turn == 0
        copies = []
        for line, sems, who in ((low, up_send, at.up), (high, down_send, at.down)):
            slot = slot_of(line, turn)
            src = w_refs[w].at[:, kept] if own_block else w_outs[w].at[slot]
            copies.append(carry(w, slot, src, sems.at[w, step, turn], who))
        return copies

    def run(flow):
        step, w, turn, low_ok, high_ok, _, _ = flow
        up_copy, down_copy = flow_copies(flow)
        if step == 0 and turn == 1:
            up_copy.wait_recv()
        if step > 0:
            pl.when(low_ok)(up_copy.wait_recv)
        pl.when(low_ok & at.has_up)(up_copy.start)
        if step > 0:
            pl.when(high_ok)(down_copy.wait_recv)
        pl.when(high_ok & at.has_down)(down_copy.start)

    for flow in flows:
        if flow[0] == 0 and flow[2] == 0:
            run(flow)
    for w in range(3):
        own.append(
            pltpu.make_async_copy(w_refs[w].at[:, kept], w_outs[w].at[at.fs], own_sem.at[w])
        )
        own[-1].start()
    for offset in range(1, at.group):
        who = at.member_id((at.member + offset) % at.group)
        for part, (src, dst) in enumerate(((late_ref, late_out), (early_ref, early_out))):
            copy = remote(
                src, dst.at[at.member], tok_send.at[part, offset], tok_recv.at[part, offset], who
            )
            copy.start()
            tokens.append(copy)
    late_out[at.member] = late_ref[...]
    early_out[at.member] = early_ref[...]
    for flow in flows:
        if not (flow[0] == 0 and flow[2] == 0):
            run(flow)
    for copy in own + tokens:
        copy.wait()
    for copy in across:
        copy.wait_send()
    for flow in flows:
        up_copy, down_copy = flow_copies(flow)
        pl.when(flow[3] & at.has_up)(up_copy.wait_send)
        pl.when(flow[4] & at.has_down)(down_copy.wait_send)


def mixed_kernel(
    n_fs,
    n_tp,
    part_ref,
    grad_ref,
    gain_ref,
    out_ref,
    pair_in,
    pair_sum,
    sums_in,
    total,
    cot,
    pair_send,
    pair_recv,
    sum_send,
    sum_recv,
    cot_send,
    cot_recv,
    relay_send,
    relay_recv,
):
    at = Place(n_fs, n_tp)
    chips = at.group // PAIR
    partner = at.member_id(at.member + 1 - 2 * at.core)
    at.enter(False)

    def chip_at(offset):
        return (at.chip + offset) % chips

    def member_at(offset):
        return chip_at(offset) * PAIR + at.core

    order = list(range(1, chips)) + [0]
    halves = {}
    for offset in order:
        theirs = chip_at(offset) * PAIR + 1 - at.core
        halves[offset] = remote(
            part_ref.at[theirs],
            pair_in.at[offset],
            pair_send.at[offset],
            pair_recv.at[offset],
            partner,
        )
        halves[offset].start()
    sums = []
    for offset in order:
        halves[offset].wait_recv()
        both = part_ref[member_at(offset)].astype(jnp.float32) + pair_in[offset].astype(jnp.float32)
        if offset == 0:
            total[...] = both
            continue
        pair_sum[offset] = both.astype(jnp.bfloat16)
        copy = remote(
            pair_sum.at[offset],
            sums_in.at[offset],
            sum_send.at[offset],
            sum_recv.at[offset],
            at.member_id(member_at(offset)),
        )
        copy.start()
        sums.append(copy)
    for offset, copy in zip(order, sums):
        copy.wait_recv()
        total[...] += sums_in[offset].astype(jnp.float32)
    mixed = total[...].astype(jnp.bfloat16).astype(jnp.float32)
    inverse = inverse_rms(mixed)
    weighted = 0.5 * grad_ref[...].astype(jnp.float32) * gain_ref[...]
    cot[...] = (
        inverse * weighted
        - mixed * inverse**3 * jnp.mean(weighted * mixed, axis=-1, keepdims=True)
    ).astype(jnp.bfloat16)
    sends = []
    for offset in order:
        who = partner if offset == 0 else at.member_id(member_at(offset))
        sends.append(
            remote(cot, out_ref.at[at.member], cot_send.at[offset], cot_recv.at[offset], who)
        )
        sends[-1].start()
    out_ref[at.member] = cot[...]
    relays = []
    for offset, copy in zip(order, sends):
        copy.wait_recv()
        if offset == 0:
            continue
        slot = member_at(chips - offset)
        relay = remote(
            out_ref.at[slot], out_ref.at[slot], relay_send.at[offset], relay_recv.at[offset], partner
        )
        relay.start()
        relays.append(relay)
    for relay in relays:
        relay.wait()
    for copy in list(halves.values()) + sums + sends:
        copy.wait_send()


def scatter_kernel(n_fs, n_tp, *refs):
    parts, tok_parts, outs, tok_outs = refs[:3], refs[3:5], refs[5:8], refs[8:10]
    below, above, given, total, tok_in = refs[10:15]
    tok_send, tok_recv, up_send, up_recv, down_send, down_recv, across_send, across_recv = refs[15:]
    at = Place(n_fs, n_tp)
    rows = parts[0].shape[1]
    piece = min(rows, 64)
    at.enter(True)

    def over_rows(body):
        @pl.loop(0, rows // piece)
        def _(i):
            body(pl.ds(pl.multiple_of(i * piece, piece), piece))

    def pass_on(w, slot, held, send, recv, is_first, who):
        def copy_from(src):
            return remote(src, held.at[w, slot], send.at[w, slot], recv.at[w, slot], who)

        @pl.when(is_first)
        def _():
            copy_from(parts[w].at[slot]).start()

        @pl.when(jnp.logical_not(is_first))
        def _():
            copy = copy_from(held.at[w, slot])
            copy.wait_recv()

            def add(span):
                held[w, slot, span] = (
                    held[w, slot, span].astype(jnp.float32)
                    + parts[w][slot, span].astype(jnp.float32)
                ).astype(jnp.bfloat16)

            over_rows(add)
            copy.start()

    def send_tokens(which):
        for offset in range(1, at.group):
            member = (at.member + offset) % at.group
            copy = remote(
                tok_parts[which].at[member],
                tok_in.at[which, offset],
                tok_send.at[which, offset],
                tok_recv.at[which, offset],
                at.member_id(member),
            )
            copy.start()
            tokens[which].append(copy)

    tokens = [[], []]
    for step in range(at.line_len - 1):
        top, bottom = at.line_len - 1 - step, step
        for w in range(3):
            for turn in range(PAIR):
                pl.when(at.line < top)(
                    functools.partial(
                        pass_on, w, top * PAIR + turn, below, up_send, up_recv,
                        at.line == 0, at.up,
                    )
                )
                pl.when(at.line > bottom)(
                    functools.partial(
                        pass_on, w, bottom * PAIR + turn, above, down_send, down_recv,
                        at.line == at.line_len - 1, at.down,
                    )
                )
                if step == 0 and w == 0 and turn == 0:
                    send_tokens(0)
                    send_tokens(1)
    for which in range(2):
        running = tok_parts[which][at.member].astype(jnp.float32)
        for offset, copy in enumerate(tokens[which], 1):
            copy.wait_recv()
            running = running + tok_in[which, offset].astype(jnp.float32)
        tok_outs[which][...] = running.astype(jnp.bfloat16)
    across = []
    for w in range(3):
        for side in (1 - at.side, at.side):
            slot = at.line * PAIR + side

            def first(span):
                total[span] = parts[w][slot, span].astype(jnp.float32)

            def arrive(held, send, recv, who):
                remote(
                    held.at[w, slot], held.at[w, slot], send.at[w, slot], recv.at[w, slot], who
                ).wait_recv()

                def add(span):
                    total[span] += held[w, slot, span].astype(jnp.float32)

                over_rows(add)

            over_rows(first)
            pl.when(at.has_down)(lambda: arrive(below, up_send, up_recv, at.up))
            pl.when(at.has_up)(lambda: arrive(above, down_send, down_recv, at.down))
            if len(across) == w:

                def give(span):
                    given[w, span] = total[span].astype(jnp.bfloat16)

                over_rows(give)
                copy = remote(
                    given.at[w], outs[w].at[at.side], across_send.at[w], across_recv.at[w], at.across
                )
                copy.start()
                across.append(copy)
            else:

                def keep(span):
                    outs[w][at.side, span] = total[span].astype(jnp.bfloat16)

                over_rows(keep)
    for copy in across:
        copy.wait()
    for copy in tokens[0] + tokens[1]:
        copy.wait_send()
    for step in range(at.line_len - 1):
        top, bottom = at.line_len - 1 - step, step
        for w in range(3):
            for turn in range(PAIR):
                up_slot, down_slot = top * PAIR + turn, bottom * PAIR + turn
                up_copy = remote(
                    below.at[w, up_slot], below.at[w, up_slot],
                    up_send.at[w, up_slot], up_recv.at[w, up_slot], at.up,
                )
                down_copy = remote(
                    above.at[w, down_slot], above.at[w, down_slot],
                    down_send.at[w, down_slot], down_recv.at[w, down_slot], at.down,
                )
                pl.when(at.line < top)(up_copy.wait_send)
                pl.when(at.line > bottom)(down_copy.wait_send)


def call(kernel, collective_id, operands, out_shapes, scratch, flops):
    in_vmem = pl.BlockSpec(memory_space=pltpu.VMEM)
    return pl.pallas_call(
        kernel,
        out_shape=out_shapes,
        in_specs=[in_vmem] * len(operands),
        out_specs=[in_vmem] * len(out_shapes),
        scratch_shapes=scratch,
        cost_estimate=pl.CostEstimate(flops=flops, bytes_accessed=0, transcendentals=0),
        compiler_params=pltpu.CompilerParams(
            collective_id=collective_id, has_side_effects=True, vmem_limit_bytes=VMEM_LIMIT
        ),
    )(*operands)


def per_device(
    n_fs,
    n_tp,
    late_input,
    early_input,
    early_grad,
    pre_gain,
    post_gain,
    gate_weight,
    up_weight,
    down_weight,
    gate_sum,
    up_sum,
    down_gradient_sum,
):
    tok_rows, model_width = late_input.shape
    shard_rows, hidden_width = gate_weight.shape
    half = hidden_width // PAIR
    group = PAIR * n_tp
    chips = group // PAIR
    line_len = n_fs // PAIR
    group_rows = group * tok_rows
    grad_scale = 1.0 / math.sqrt(tok_rows * n_tp * n_fs)
    dma = pltpu.SemaphoreType.DMA
    bf16 = jnp.bfloat16

    def shaped(*shape):
        return jax.ShapeDtypeStruct(shape, bf16)

    def normed_of(rows):
        values = rows.astype(jnp.float32)
        inverse = inverse_rms(values)
        return values, inverse, (values * inverse * pre_gain).astype(bf16)

    late_values, _, late_normed = normed_of(late_input)
    early_values, early_in_inverse, early_own = normed_of(early_input)
    tok_block = shaped(group, tok_rows, model_width)
    w_block = shaped(n_fs, shard_rows, half)
    late_rows, early_rows, gate_all, up_all, down_all = call(
        functools.partial(gather_kernel, n_fs, n_tp),
        0,
        (late_normed, early_own, gate_weight, up_weight, down_weight),
        [tok_block, tok_block, w_block, w_block, w_block],
        [
            dma((2, group)),
            dma((2, group)),
            dma((3,)),
            dma((3,)),
            dma((3, line_len, PAIR)),
            dma((3, line_len, PAIR)),
            dma((3, n_fs)),
        ],
        10**9,
    )
    late_rows = late_rows.reshape(group_rows, model_width)
    early_rows = early_rows.reshape(group_rows, model_width)
    gate_all, up_all, down_all = (
        full.reshape(model_width, half) for full in (gate_all, up_all, down_all)
    )

    def hidden_of(rows):
        gate_pre = jnp.dot(rows, gate_all, preferred_element_type=jnp.float32)
        up_pre = jnp.dot(rows, up_all, preferred_element_type=jnp.float32)
        return gate_pre, up_pre, (jax.nn.silu(gate_pre) * up_pre).astype(bf16)

    def by_owner(product):
        return product.astype(bf16).reshape(group, tok_rows, model_width)

    early_gate, early_up, early_hidden = hidden_of(early_rows)
    early_part = by_owner(contract_last(early_hidden, down_all))
    chip_block = pltpu.VMEM((chips, tok_rows, model_width), bf16)
    (cot_rows,) = call(
        functools.partial(mixed_kernel, n_fs, n_tp),
        1,
        (early_part, early_grad, post_gain.reshape(1, model_width)),
        [tok_block],
        [
            chip_block,
            chip_block,
            chip_block,
            pltpu.VMEM((tok_rows, model_width), jnp.float32),
            pltpu.VMEM((tok_rows, model_width), bf16),
        ]
        + [dma((chips,))] * 8,
        10**8,
    )
    cot_rows = cot_rows.reshape(group_rows, model_width)
    _, _, late_hidden = hidden_of(late_rows)
    late_part = by_owner(contract_last(late_hidden, down_all))
    hidden_cot = jnp.dot(cot_rows, down_all, preferred_element_type=jnp.float32)
    sigmoid_gate = jax.nn.sigmoid(early_gate)
    gate_cot = (
        hidden_cot * early_up * sigmoid_gate * (1.0 + early_gate * (1.0 - sigmoid_gate))
    ).astype(bf16)
    up_cot = (hidden_cot * early_gate * sigmoid_gate).astype(bf16)
    normed_part = by_owner(contract_last(gate_cot, gate_all) + contract_last(up_cot, up_all))
    grad_parts = [
        (grad_scale * contract_first(first_op, second_op))
        .astype(bf16)
        .reshape(n_fs, shard_rows, half)
        for first_op, second_op in (
            (early_rows, gate_cot),
            (early_rows, up_cot),
            (cot_rows, early_hidden),
        )
    ]
    own_tokens = shaped(tok_rows, model_width)
    own_shard = shaped(PAIR, shard_rows, half)
    line_block = pltpu.VMEM((3, n_fs, shard_rows, half), bf16)
    *grads, normed_cot, late_mixed = call(
        functools.partial(scatter_kernel, n_fs, n_tp),
        2,
        (*grad_parts, normed_part, late_part),
        [own_shard, own_shard, own_shard, own_tokens, own_tokens],
        [
            line_block,
            line_block,
            pltpu.VMEM((3, shard_rows, half), bf16),
            pltpu.VMEM((shard_rows, half), jnp.float32),
            pltpu.VMEM((2, group, tok_rows, model_width), bf16),
            dma((2, group)),
            dma((2, group)),
        ]
        + [dma((3, n_fs))] * 4
        + [dma((3,))] * 2,
        10**9,
    )
    late_mixed = late_mixed.astype(jnp.float32)
    late_output = (
        late_values + 0.5 * late_mixed * inverse_rms(late_mixed) * post_gain
    ).astype(bf16)
    weighted_in = normed_cot.astype(jnp.float32) * pre_gain
    early_input_grad = (
        early_grad.astype(jnp.float32)
        + early_in_inverse * weighted_in
        - early_values
        * early_in_inverse**3
        * jnp.mean(weighted_in * early_values, axis=-1, keepdims=True)
    ).astype(bf16)
    totals = [
        running + jnp.concatenate([grad[0], grad[1]], axis=1).astype(jnp.float32)
        for running, grad in zip((gate_sum, up_sum, down_gradient_sum), grads)
    ]
    return (late_output, early_input_grad, *totals)


def solution(mesh):
    in_specs = (
        P(("fs", "tp"), None),
        P(("fs", "tp"), None),
        P(("fs", "tp"), None),
        P(),
        P(),
        P("fs", "tp"),
        P("fs", "tp"),
        P("fs", "tp"),
        P("fs", "tp"),
        P("fs", "tp"),
        P("fs", "tp"),
    )
    out_specs = (
        P(("fs", "tp"), None),
        P(("fs", "tp"), None),
        P("fs", "tp"),
        P("fs", "tp"),
        P("fs", "tp"),
    )
    return jax.shard_map(
        functools.partial(per_device, mesh.shape["fs"], mesh.shape["tp"]),
        mesh=mesh, in_specs=in_specs, out_specs=out_specs, check_vma=False
    )
```

time: 586 us -> 324 us (0.55)
  waiting for transfers between devices: 492 us -> 0 us
  Pallas kernels: 0 us -> 276 us
  local copies, waits for them, and re-layouts: 22.5 us -> 1.56 us
  between operations: 14.4 us -> 0.84 us
  other arithmetic: 20.5 us -> 9.88 us
    pallas_call x0 -> x3, Pallas kernels: none -> 276 us  [call(): pl.pallas_call(kernel, out_shape=out_shapes, in_specs=[in_vmem] * len(ope...]
    all_gather x5 -> x0, waiting for transfers between devices: 246 us -> none  [the longest x1 74.4 us: per_device(): lax.all_gather(gate_weight, 'fs', axis=0, tiled=True)]
    reduce_scatter x2 -> x0, waiting for transfers between devices: 214 us -> none  [the longest x1 207 us: per_device(): lax.psum_scatter((grad_scale * jnp.concatenate([contract_first(early_norm...]
    unnamed x9 -> x0, waiting for transfers between devices: 32.3 us -> none
    unnamed x43 -> x36, local copies, waits for them, and re-layouts: 16.7 us -> 0.36 us
    convert_element_type x5 -> x2, other arithmetic: 13.3 us -> 2.89 us  [the longest x1 2.02 us: normed_of(): return (values, inverse, (values * inverse * pre_gain).astype(bf16))]
    dot_general x4, matrix products: 23.8 us -> 13.7 us  [the longest x2 7.23 us: hidden_of(): gate_pre = jnp.dot(rows, gate_all, preferred_element_type=jnp.float32)]
    dot_general x2 -> x4, matrix products: 3.56 us -> 12.6 us  [contract_last(): lax.dot_general(first_op, second_op, (((1,), (1,)), ((), ())), preferred_...]
  transfers between devices with their start and end apart: 8 -> 0, of which waited for: 8 -> 0; matrix products, arithmetic and copies ran while one was open for 6% -> 0% of each run, Pallas kernels for 0% -> 0%
where the time goes in v1:
time: 324 us; the launch traced here: 323 us
  Pallas kernels  276 us (85%)
  matrix products  34.3 us (11%)
  other arithmetic  9.88 us (3%)
    pallas_call x3, Pallas kernels, call(): pl.pallas_call(kernel, out_shape=out_shapes, in_specs=[in_vmem] * len(ope...  276 us
    dot_general x4, matrix products, contract_last(): lax.dot_general(first_op, second_op, (((1,), (1,)), ((), ())), preferred_...  12.6 us
    dot_general x3, matrix products, contract_first(): lax.dot_general(first_op, second_op, (((0,), (0,)), ((), ())), preferred_...  8.11 us
    dot_general x2, matrix products, hidden_of(): gate_pre = jnp.dot(rows, gate_all, preferred_element_type=jnp.float32)  7.23 us

profile of v1, /device:TPU:16, one launch (start us, length us, event | category | flops | bytes accessed | tf_op | source)
XLA Modules:
  0.0 323.1 jit_solution(4693279891043598450)
XLA Ops:
  0.6 1.1 fusion.3
  1.7 1.1 fusion.7
  2.9 2.0 fusion.9
  4.9 122.6 %shard_map.146 = (bf16[8,64,2048]{2,1,0:T(8,128)(2,1)}, bf16[8,64,2048]{2,1,0:T(8,128)(2,1)}, bf16[8,256,512]{2,1,0:T(8,128)(2,1)}, bf16[8,256,512]{2,1,0:T(8,128)(2,1)}, bf16[8,256,512]{2,1,0:T(8,128)(2,1)}) custom-call(bf16[64,2048]{1,0:T(8,128)(2,1)} %get-tuple-element.34.late_ref, bf16[64,2048]{1,0:T(8,128)(2,1)} %get-tuple-element.33.early_ref, ...), custom_call_target="tpu_custom_call" | custom-call | flops 1000000000 | tf_op jit(solution)/shard_map/pallas_call | solution.py:399
  127.5 0.0 copy-start.2
  127.5 3.6 %fusion.18 = f32[512,512]{1,0:T(8,128)S(1)} fusion(bf16[512,2048]{1,0:T(8,128)(2,1)} %bitcast.70, bf16[2048,512]{1,0:T(8,128)(2,1)} %bitcast.59), kind=kOutput, calls=%fused_computation.53 | convolution fusion | flops 1073741824 | bytes 5242880 | tf_op jit(solution)/shard_map/dot_general | solution.py:473
  131.1 0.0 copy-done.2
  131.1 6.0 %convolution_convert_fusion = bf16[512,2048]{1,0:T(8,128)(2,1)} fusion(bf16[2048,512]{1,0:T(8,128)(2,1)} %bitcast.67, bf16[512,2048]{1,0:T(8,128)(2,1)} %bitcast.71, bf16[2048,512]{1,0:T(8,128)(2,1)S(1)} %bitcast.50, f32[512,512]{1,0:T(8,128)S(1)} %fusion.18), kind=kOutput, calls=%fused_computation.4 | convolution fusion | flops 2150105088 | bytes 9437184 | tf_op jit(solution)/shard_map/dot_general | solution.py:18
  137.1 3.6 %fusion.16 = f32[512,512]{1,0:T(8,128)S(1)} fusion(bf16[512,2048]{1,0:T(8,128)(2,1)} %bitcast.63, bf16[2048,512]{1,0:T(8,128)(2,1)} %bitcast.60), kind=kOutput, calls=%fused_computation.51 | convolution fusion | flops 1073741824 | bytes 5242880 | tf_op jit(solution)/shard_map/dot_general | solution.py:473
  140.8 0.0 copy-done.15
  140.8 0.0 copy-start.17
  140.8 2.3 multiply_convert_fusion.5
  143.0 0.0 copy-done.17
  143.0 2.7 convolution_convert_fusion.1
  145.7 35.2 %shard_map.147 = bf16[8,64,2048]{2,1,0:T(8,128)(2,1)} custom-call(bf16[8,64,2048]{2,1,0:T(8,128)(2,1)} %bitcast.58, bf16[64,2048]{1,0:T(8,128)(2,1)} %grad_ref.1, f32[1,2048]{1,0:T(1,128)} %bitcast.62), custom_call_target="tpu_custom_call" | custom-call | flops 100000000 | tf_op jit(solution)/shard_map/pallas_call | solution.py:399
  180.9 0.0 copy-start.4
  180.9 4.2 %multiply_convert_fusion.3 = (bf16[512,512]{1,0:T(8,128)(2,1)S(1)}, bf16[512,512]{1,0:T(8,128)(2,1)S(1)}) fusion(f32[512,512]{1,0:T(8,128)S(1)} %fusion.16, f32[512,512]{1,0:T(8,128)} %get-tuple-element.38, bf16[512,2048]{1,0:T(8,128)(2,1)} %bitcast.56, bf16[2048,512]{1,0:T(8,128)(2,1)} %bitcast.68), kind=kOutput, calls=%fused_computation.11 | convolution fusion | flops 1077149696 | bytes 7340032 | tf_op jit(solution)/shard_map/dot_general | solution.py:501
  185.1 0.0 copy-done.4
  185.1 1.3 fusion.17
  186.4 0.0 copy-start.3
  186.4 2.6 add_convert_fusion
  189.0 0.0 copy-done.3
  189.0 2.6 multiply_convert_fusion
  191.7 0.0 copy-done.16
  191.7 2.7 multiply_convert_fusion.1
  194.4 2.8 multiply_convert_fusion.2
  197.2 118.6 %shard_map.148 = (bf16[2,256,512]{2,1,0:T(8,128)(2,1)}, bf16[2,256,512]{2,1,0:T(8,128)(2,1)}, bf16[2,256,512]{2,1,0:T(8,128)(2,1)}, bf16[64,2048]{1,0:T(8,128)(2,1)}, bf16[64,2048]{1,0:T(8,128)(2,1)}) custom-call(bf16[8,256,512]{2,1,0:T(8,128)(2,1)} %bitcast.55, bf16[8,256,512]{2,1,0:T(8,128)(2,1)} %bitcast.54, bf16[8,256,512]{2,1,0:T(8,128)(2,1)} %bitcast.53, ...), custom_call_target="tpu_custom_call" | custom-call | flops 1000000000 | tf_op jit(solution)/shard_map/pallas_call | solution.py:399
  315.8 0.0 copy-start.12
  315.8 1.1 slice_bitcast_fusion.1
  316.9 0.0 copy-start.8
  316.9 0.0 copy-done.7
  317.0 1.2 convert_add_fusion
  318.1 0.0 copy-done.12
  318.2 0.0 copy-start.9
  318.2 0.2 copy-done.8
  318.4 1.1 convert_add_fusion.1
  319.5 0.0 copy-done.11
  319.5 0.0 copy-start.5
  319.6 0.0 copy-done.9
  319.6 1.2 convert_add_fusion.2
  320.8 0.0 copy-done
  320.8 0.0 copy-done.6
  320.8 0.0 copy-done.13
  320.8 0.2 fusion.13
  321.0 1.0 fusion.12
  322.0 0.2 fusion.1
  322.2 0.0 copy-done.14
  322.2 0.9 fusion.6
  (18 shorter events, 0.1 us)
Async XLA Ops:
  127.5 3.6 %copy-start.2 = (bf16[8,256,512]{2,1,0:T(8,128)(2,1)S(1)}, bf16[8,256,512]{2,1,0:T(8,128)(2,1)}, u32[]{:S(2)}) copy-start(bf16[8,256,512]{2,1,0:T(8,128)(2,1)} %get-tuple-element.17) | copy-start | bytes 6291460
  137.1 3.6 %copy-start.15 = (bf16[8,64,2048]{2,1,0:T(8,128)(2,1)S(1)}, bf16[8,64,2048]{2,1,0:T(8,128)(2,1)}, u32[]{:S(2)}) copy-start(bf16[8,64,2048]{2,1,0:T(8,128)(2,1)} %get-tuple-element.15) | copy-start | bytes 6291460
  140.8 2.3 copy-start.17
  180.9 4.2 %copy-start.4 = (bf16[8,256,512]{2,1,0:T(8,128)(2,1)S(1)}, bf16[8,256,512]{2,1,0:T(8,128)(2,1)}, u32[]{:S(2)}) copy-start(bf16[8,256,512]{2,1,0:T(8,128)(2,1)} %get-tuple-element.16) | copy-start | bytes 6291460
  186.4 2.6 copy-start.3
  189.0 2.6 copy-start.16
  197.2 119.8 %copy-start.7 = (f32[256,1024]{1,0:T(8,128)S(1)}, f32[256,1024]{1,0:T(8,128)}, u32[]{:S(2)}) copy-start(f32[256,1024]{1,0:T(8,128)} %param.21) | copy-start | bytes 3145732
  315.8 2.3 copy-start.12
  316.9 1.5 copy-start.8
  318.1 1.4 copy-start.11
  318.2 1.5 copy-start.9
  319.5 1.3 copy-start
  319.5 1.3 copy-start.6
  319.5 1.3 copy-start.13
  319.5 1.5 copy-start.5
  319.6 2.4 copy-start.10
  319.6 2.5 copy-start.1
  319.6 2.5 copy-start.14

commit v2 on v1

--- a/solution.py
+++ b/solution.py
@@ -141,6 +141,11 @@
             pltpu.make_async_copy(w_refs[w].at[:, kept], w_outs[w].at[at.fs], own_sem.at[w])
         )
         own[-1].start()
+    late_out[at.member] = late_ref[...]
+    early_out[at.member] = early_ref[...]
+    for flow in flows:
+        if flow[0] == 0 and flow[2] == 1:
+            run(flow)
     for offset in range(1, at.group):
         who = at.member_id((at.member + offset) % at.group)
         for part, (src, dst) in enumerate(((late_ref, late_out), (early_ref, early_out))):
@@ -149,10 +154,8 @@
             )
             copy.start()
             tokens.append(copy)
-    late_out[at.member] = late_ref[...]
-    early_out[at.member] = early_ref[...]
     for flow in flows:
-        if not (flow[0] == 0 and flow[2] == 0):
+        if flow[0] > 0:
             run(flow)
     for copy in own + tokens:
         copy.wait()
@@ -260,13 +263,34 @@
         copy.wait_send()
 
 
-def scatter_kernel(n_fs, n_tp, *refs):
-    parts, tok_parts, outs, tok_outs = refs[:3], refs[3:5], refs[5:8], refs[8:10]
-    below, above, given, total, tok_in = refs[10:15]
-    tok_send, tok_recv, up_send, up_recv, down_send, down_recv, across_send, across_recv = refs[15:]
+def scatter_kernel(n_fs, n_tp, grad_scale, *refs):
+    cot_ref, hidden_ref = refs[:2]
+    outs, tok_outs = refs[9:12], refs[12:14]
+    staged = refs[14:21]
+    early_ref, down_ref, gate_ref, up_ref, gate_w, up_w, late_ref = staged
+    parts, below, above, given, total, gate_cot, up_cot, tok_parts, tok_in = refs[21:30]
+    (
+        stage_sem,
+        tok_send,
+        tok_recv,
+        up_send,
+        up_recv,
+        down_send,
+        down_recv,
+        across_send,
+        across_recv,
+    ) = refs[30:]
     at = Place(n_fs, n_tp)
-    rows = parts[0].shape[1]
+    rows, tok_rows = parts.shape[2], tok_parts.shape[2]
     piece = min(rows, 64)
+    owners = min(at.group, 4)
+    tile = owners * tok_rows
+    loads = [
+        pltpu.make_async_copy(src, dst, stage_sem.at[i])
+        for i, (src, dst) in enumerate(zip(refs[2:9], staged))
+    ]
+    for load in loads:
+        load.start()
     at.enter(True)
 
     def over_rows(body):
@@ -274,33 +298,73 @@
         def _(i):
             body(pl.ds(pl.multiple_of(i * piece, piece), piece))
 
-    def pass_on(w, slot, held, send, recv, is_first, who):
-        def copy_from(src):
-            return remote(src, held.at[w, slot], send.at[w, slot], recv.at[w, slot], who)
-
-        @pl.when(is_first)
+    def over_tokens(body):
+        @pl.loop(0, at.group // owners)
+        def _(i):
+            body(pl.ds(pl.multiple_of(i * tile, tile), tile), pl.ds(i * owners, owners))
+
+    def grad_part(w, left_ref, right_ref):
+        @pl.loop(0, n_fs)
+        def _(slot):
+            left = left_ref[:, pl.ds(pl.multiple_of(slot * rows, rows), rows)]
+            parts[w, slot] = (grad_scale * contract_first(left, right_ref[...])).astype(
+                jnp.bfloat16
+            )
+
+    def slots_of(w):
+        for step in range(at.line_len - 1):
+            for turn in range(PAIR):
+                side = 1 - at.side if turn == 0 else at.side
+                top, bottom = at.line_len - 1 - step, step
+                yield top, top * PAIR + side, bottom, bottom * PAIR + side
+
+    def hop(w, slot, src, upward):
+        held, send, recv, who = (
+            (below, up_send, up_recv, at.up) if upward else (above, down_send, down_recv, at.down)
+        )
+        src = held.at[w, slot] if src is None else src
+        return remote(src, held.at[w, slot], send.at[w, slot], recv.at[w, slot], who)
+
+    def first_sends(w):
+        @pl.when(at.line == 0)
         def _():
-            copy_from(parts[w].at[slot]).start()
-
-        @pl.when(jnp.logical_not(is_first))
+            for _, slot, _, _ in slots_of(w):
+                hop(w, slot, parts.at[w, slot], True).start()
+
+        @pl.when(at.line == at.line_len - 1)
         def _():
-            copy = copy_from(held.at[w, slot])
-            copy.wait_recv()
-
-            def add(span):
-                held[w, slot, span] = (
-                    held[w, slot, span].astype(jnp.float32)
-                    + parts[w][slot, span].astype(jnp.float32)
-                ).astype(jnp.bfloat16)
-
-            over_rows(add)
-            copy.start()
+            for _, _, _, slot in slots_of(w):
+                hop(w, slot, parts.at[w, slot], False).start()
+
+    def pass_on(w, slot, upward):
+        copy = hop(w, slot, None, upward)
+        held = below if upward else above
+        copy.wait_recv()
+
+        def add(span):
+            held[w, slot, span] = (
+                held[w, slot, span].astype(jnp.float32) + parts[w, slot, span].astype(jnp.float32)
+            ).astype(jnp.bfloat16)
+
+        over_rows(add)
+        copy.start()
+
+    def middle_sends(w):
+        for top, up_slot, bottom, down_slot in slots_of(w):
+            pl.when((at.line > 0) & (at.line < top))(
+                functools.partial(pass_on, w, up_slot, True)
+            )
+            pl.when((at.line < at.line_len - 1) & (at.line > bottom))(
+                functools.partial(pass_on, w, down_slot, False)
+            )
+
+    tokens = [[], []]
 
     def send_tokens(which):
         for offset in range(1, at.group):
             member = (at.member + offset) % at.group
             copy = remote(
-                tok_parts[which].at[member],
+                tok_parts.at[which, member],
                 tok_in.at[which, offset],
                 tok_send.at[which, offset],
                 tok_recv.at[which, offset],
@@ -309,44 +373,43 @@
             copy.start()
             tokens[which].append(copy)
 
-    tokens = [[], []]
-    for step in range(at.line_len - 1):
-        top, bottom = at.line_len - 1 - step, step
-        for w in range(3):
-            for turn in range(PAIR):
-                pl.when(at.line < top)(
-                    functools.partial(
-                        pass_on, w, top * PAIR + turn, below, up_send, up_recv,
-                        at.line == 0, at.up,
-                    )
-                )
-                pl.when(at.line > bottom)(
-                    functools.partial(
-                        pass_on, w, bottom * PAIR + turn, above, down_send, down_recv,
-                        at.line == at.line_len - 1, at.down,
-                    )
-                )
-                if step == 0 and w == 0 and turn == 0:
-                    send_tokens(0)
-                    send_tokens(1)
-    for which in range(2):
-        running = tok_parts[which][at.member].astype(jnp.float32)
-        for offset, copy in enumerate(tokens[which], 1):
-            copy.wait_recv()
-            running = running + tok_in[which, offset].astype(jnp.float32)
-        tok_outs[which][...] = running.astype(jnp.bfloat16)
+    def by_owner(product):
+        return product.astype(jnp.bfloat16).reshape(owners, tok_rows, product.shape[-1])
+
+    def cots(span, _):
+        hidden_cot = jnp.dot(cot_ref[span], down_ref[...], preferred_element_type=jnp.float32)
+        gate, up = gate_ref[span], up_ref[span]
+        sigmoid = jax.nn.sigmoid(gate)
+        gate_cot[span] = (hidden_cot * up * sigmoid * (1.0 + gate * (1.0 - sigmoid))).astype(
+            jnp.bfloat16
+        )
+        up_cot[span] = (hidden_cot * gate * sigmoid).astype(jnp.bfloat16)
+
+    def normed_part(span, owned):
+        tok_parts[0, owned] = by_owner(
+            contract_last(gate_cot[span], gate_w[...]) + contract_last(up_cot[span], up_w[...])
+        )
+
+    def late_part(span, owned):
+        late = late_ref[span]
+        gate = jnp.dot(late, gate_w[...], preferred_element_type=jnp.float32)
+        up = jnp.dot(late, up_w[...], preferred_element_type=jnp.float32)
+        hidden = (gate * jax.nn.sigmoid(gate) * up).astype(jnp.bfloat16)
+        tok_parts[1, owned] = by_owner(contract_last(hidden, down_ref[...]))
+
     across = []
-    for w in range(3):
-        for side in (1 - at.side, at.side):
+
+    def finish(w):
+        for turn in range(PAIR):
+            side = 1 - at.side if turn == 0 else at.side
             slot = at.line * PAIR + side
 
             def first(span):
-                total[span] = parts[w][slot, span].astype(jnp.float32)
-
-            def arrive(held, send, recv, who):
-                remote(
-                    held.at[w, slot], held.at[w, slot], send.at[w, slot], recv.at[w, slot], who
-                ).wait_recv()
+                total[span] = parts[w, slot, span].astype(jnp.float32)
+
+            def arrive(upward):
+                held = below if upward else above
+                hop(w, slot, None, upward).wait_recv()
 
                 def add(span):
                     total[span] += held[w, slot, span].astype(jnp.float32)
@@ -354,9 +417,9 @@
                 over_rows(add)
 
             over_rows(first)
-            pl.when(at.has_down)(lambda: arrive(below, up_send, up_recv, at.up))
-            pl.when(at.has_up)(lambda: arrive(above, down_send, down_recv, at.down))
-            if len(across) == w:
+            pl.when(at.has_down)(functools.partial(arrive, True))
+            pl.when(at.has_up)(functools.partial(arrive, False))
+            if turn == 0:
 
                 def give(span):
                     given[w, span] = total[span].astype(jnp.bfloat16)
@@ -373,33 +436,52 @@
                     outs[w][at.side, span] = total[span].astype(jnp.bfloat16)
 
                 over_rows(keep)
+
+    grad_part(2, cot_ref, hidden_ref)
+    first_sends(2)
+    for load in loads[:4]:
+        load.wait()
+    over_tokens(cots)
+    grad_part(0, early_ref, gate_cot)
+    first_sends(0)
+    grad_part(1, early_ref, up_cot)
+    first_sends(1)
+    for load in loads[4:]:
+        load.wait()
+    over_tokens(normed_part)
+    send_tokens(0)
+    middle_sends(2)
+    over_tokens(late_part)
+    send_tokens(1)
+    middle_sends(0)
+    finish(2)
+    for which in range(2):
+        running = tok_parts[which, at.member].astype(jnp.float32)
+        for offset, copy in enumerate(tokens[which], 1):
+            copy.wait_recv()
+            running = running + tok_in[which, offset].astype(jnp.float32)
+        tok_outs[which][...] = running.astype(jnp.bfloat16)
+        if which == 0:
+            middle_sends(1)
+            finish(0)
+    finish(1)
     for copy in across:
         copy.wait()
     for copy in tokens[0] + tokens[1]:
         copy.wait_send()
-    for step in range(at.line_len - 1):
-        top, bottom = at.line_len - 1 - step, step
-        for w in range(3):
-            for turn in range(PAIR):
-                up_slot, down_slot = top * PAIR + turn, bottom * PAIR + turn
-                up_copy = remote(
-                    below.at[w, up_slot], below.at[w, up_slot],
-                    up_send.at[w, up_slot], up_recv.at[w, up_slot], at.up,
-                )
-                down_copy = remote(
-                    above.at[w, down_slot], above.at[w, down_slot],
-                    down_send.at[w, down_slot], down_recv.at[w, down_slot], at.down,
-                )
-                pl.when(at.line < top)(up_copy.wait_send)
-                pl.when(at.line > bottom)(down_copy.wait_send)
-
-
-def call(kernel, collective_id, operands, out_shapes, scratch, flops):
+    for w in range(3):
+        for top, up_slot, bottom, down_slot in slots_of(w):
+            pl.when(at.line < top)(hop(w, up_slot, None, True).wait_send)
+            pl.when(at.line > bottom)(hop(w, down_slot, None, False).wait_send)
+
+
+def call(kernel, collective_id, operands, out_shapes, scratch, flops, n_any=0):
     in_vmem = pl.BlockSpec(memory_space=pltpu.VMEM)
+    in_any = pl.BlockSpec(memory_space=pl.ANY)
     return pl.pallas_call(
         kernel,
         out_shape=out_shapes,
-        in_specs=[in_vmem] * len(operands),
+        in_specs=[in_vmem] * (len(operands) - n_any) + [in_any] * n_any,
         out_specs=[in_vmem] * len(out_shapes),
         scratch_shapes=scratch,
         cost_estimate=pl.CostEstimate(flops=flops, bytes_accessed=0, transcendentals=0),
@@ -496,45 +578,34 @@
         10**8,
     )
     cot_rows = cot_rows.reshape(group_rows, model_width)
-    _, _, late_hidden = hidden_of(late_rows)
-    late_part = by_owner(contract_last(late_hidden, down_all))
-    hidden_cot = jnp.dot(cot_rows, down_all, preferred_element_type=jnp.float32)
-    sigmoid_gate = jax.nn.sigmoid(early_gate)
-    gate_cot = (
-        hidden_cot * early_up * sigmoid_gate * (1.0 + early_gate * (1.0 - sigmoid_gate))
-    ).astype(bf16)
-    up_cot = (hidden_cot * early_gate * sigmoid_gate).astype(bf16)
-    normed_part = by_owner(contract_last(gate_cot, gate_all) + contract_last(up_cot, up_all))
-    grad_parts = [
-        (grad_scale * contract_first(first_op, second_op))
-        .astype(bf16)
-        .reshape(n_fs, shard_rows, half)
-        for first_op, second_op in (
-            (early_rows, gate_cot),
-            (early_rows, up_cot),
-            (cot_rows, early_hidden),
-        )
-    ]
+    staged = (early_rows, down_all, early_gate, early_up, gate_all, up_all, late_rows)
     own_tokens = shaped(tok_rows, model_width)
     own_shard = shaped(PAIR, shard_rows, half)
     line_block = pltpu.VMEM((3, n_fs, shard_rows, half), bf16)
     *grads, normed_cot, late_mixed = call(
-        functools.partial(scatter_kernel, n_fs, n_tp),
+        functools.partial(scatter_kernel, n_fs, n_tp, grad_scale),
         2,
-        (*grad_parts, normed_part, late_part),
+        (cot_rows, early_hidden, *staged),
         [own_shard, own_shard, own_shard, own_tokens, own_tokens],
-        [
+        [pltpu.VMEM(array.shape, array.dtype) for array in staged]
+        + [
+            line_block,
             line_block,
             line_block,
             pltpu.VMEM((3, shard_rows, half), bf16),
             pltpu.VMEM((shard_rows, half), jnp.float32),
+            pltpu.VMEM((group_rows, half), bf16),
+            pltpu.VMEM((group_rows, half), bf16),
             pltpu.VMEM((2, group, tok_rows, model_width), bf16),
+            pltpu.VMEM((2, group, tok_rows, model_width), bf16),
+            dma((len(staged),)),
             dma((2, group)),
             dma((2, group)),
         ]
         + [dma((3, n_fs))] * 4
         + [dma((3,))] * 2,
         10**9,
+        n_any=len(staged),
     )
     late_mixed = late_mixed.astype(jnp.float32)
     late_output = (

time: 324 us -> 294 us (0.907)
  matrix products: 34.3 us -> 8.52 us
  Pallas kernels: 276 us -> 271 us
    dot_general x4 -> x0, matrix products: 12.3 us -> none  [the longest x3 8.11 us: contract_first(): lax.dot_general(first_op, second_op, (((0,), (0,)), ((), ())), preferred_...]
    dot_general x4 -> x1, matrix products: 12.6 us -> 2.65 us  [contract_last(): lax.dot_general(first_op, second_op, (((1,), (1,)), ((), ())), preferred_...]
    pallas_call x3, Pallas kernels: 276 us -> 271 us  [call(): pl.pallas_call(kernel, out_shape=out_shapes, in_specs=[in_vmem] * (len(op...]
    dot_general x2 -> x1, matrix products: 7.23 us -> 3.62 us  [hidden_of(): gate_pre = jnp.dot(rows, gate_all, preferred_element_type=jnp.float32)]
where the time goes in v2:
time: 294 us; the launch traced here: 293 us
  Pallas kernels  271 us (92%)
  other arithmetic  11.7 us (4%)
  matrix products  8.52 us (3%)
    pallas_call x3, Pallas kernels, call(): pl.pallas_call(kernel, out_shape=out_shapes, in_specs=[in_vmem] * (len(op...  271 us

profile of v2, /device:TPU:16, one launch (start us, length us, event | category | flops | bytes accessed | tf_op | source)
XLA Modules:
  0.0 293.4 jit_solution(7520291370629000966)
XLA Ops:
  0.6 1.1 fusion.2
  1.7 1.1 fusion.6
  2.9 2.0 fusion.8
  4.9 110.5 %shard_map.146 = (bf16[8,64,2048]{2,1,0:T(8,128)(2,1)}, bf16[8,64,2048]{2,1,0:T(8,128)(2,1)}, bf16[8,256,512]{2,1,0:T(8,128)(2,1)}, bf16[8,256,512]{2,1,0:T(8,128)(2,1)}, bf16[8,256,512]{2,1,0:T(8,128)(2,1)}) custom-call(bf16[64,2048]{1,0:T(8,128)(2,1)} %get-tuple-element.32.late_ref, bf16[64,2048]{1,0:T(8,128)(2,1)} %get-tuple-element.31.early_ref, ...), custom_call_target="tpu_custom_call" | custom-call | flops 1000000000 | tf_op jit(solution)/shard_map/pallas_call | solution.py:481
  115.4 0.0 copy-start.2
  115.4 0.0 copy-start.3
  115.4 3.6 %fusion.13.refs_4_ = f32[512,512]{1,0:T(8,128)S(1)} fusion(bf16[512,2048]{1,0:T(8,128)(2,1)} %bitcast.29, bf16[2048,512]{1,0:T(8,128)(2,1)} %bitcast.32), kind=kOutput, calls=%fused_computation.39 | convolution fusion | flops 1073741824 | bytes 5242880 | tf_op jit(solution)/shard_map/dot_general | solution.py:555
  119.1 0.0 copy-done.2
  119.1 0.0 copy-done.3
  119.1 0.0 copy-start.10
  119.1 0.0 copy-start.4
  119.1 2.3 multiply_convert_fusion
  121.4 0.0 copy-done.10
  121.4 0.0 copy-start.13
  121.4 0.0 copy-done.4
  121.4 2.7 convolution_convert_fusion
  124.0 0.0 copy-done.13
  124.0 34.4 %shard_map.147 = bf16[8,64,2048]{2,1,0:T(8,128)(2,1)} custom-call(bf16[8,64,2048]{2,1,0:T(8,128)(2,1)} %bitcast.27, bf16[64,2048]{1,0:T(8,128)(2,1)} %grad_ref.1, f32[1,2048]{1,0:T(1,128)} %bitcast.38), custom_call_target="tpu_custom_call" | custom-call | flops 100000000 | tf_op jit(solution)/shard_map/pallas_call | solution.py:481
  158.4 0.0 copy-start.1
  158.4 0.0 copy-start.15
  158.4 125.7 %shard_map.148 = (bf16[2,256,512]{2,1,0:T(8,128)(2,1)}, bf16[2,256,512]{2,1,0:T(8,128)(2,1)}, bf16[2,256,512]{2,1,0:T(8,128)(2,1)}, bf16[64,2048]{1,0:T(8,128)(2,1)}, bf16[64,2048]{1,0:T(8,128)(2,1)}) custom-call(bf16[512,2048]{1,0:T(8,128)(2,1)} %bitcast.26, bf16[512,512]{1,0:T(8,128)(2,1)} %copy-done.13, bf16[512,2048]{1,0:T(8,128)(2,1)} %bitcast.30, ...), custom_call_target="tpu_custom_call" | custom-call | flops 1000000000 | tf_op jit(solution)/shard_map/pallas_call | solution.py:481
  284.1 0.0 copy-start
  284.1 0.0 copy-start.6
  284.1 0.0 copy-start.14
  284.1 0.0 copy-start.5
  284.1 0.0 copy-start.7
  284.2 1.2 slice_bitcast_fusion.5
  285.4 1.1 fusion
  286.5 0.0 copy-done.1
  286.5 0.0 copy-done.15
  286.5 1.8 fusion.5
  288.3 0.0 copy-done
  288.3 0.0 copy-done.6
  288.3 0.0 copy-done.14
  288.3 0.0 copy-start.12
  288.3 0.2 fusion.12
  288.5 0.0 copy-done.5
  288.5 1.0 fusion.11
  289.5 0.0 copy-done.7
  289.5 0.0 copy-start.8
  289.5 1.1 convert_add_fusion.2
  290.6 0.0 copy-done.12
  290.7 0.0 copy-start.9
  290.7 0.4 copy-done.8
  291.1 1.1 convert_add_fusion.1
  292.2 0.0 copy-done.11
  292.3 0.0 copy-done.9
  292.3 1.1 convert_add_fusion
  (6 shorter events, 0.1 us)
Async XLA Ops:
  115.4 3.6 %copy-start.2 = (bf16[8,64,2048]{2,1,0:T(8,128)(2,1)S(1)}, bf16[8,64,2048]{2,1,0:T(8,128)(2,1)}, u32[]{:S(2)}) copy-start(bf16[8,64,2048]{2,1,0:T(8,128)(2,1)} %get-tuple-element.15) | copy-start | bytes 6291460
  115.4 3.6 %copy-start.3 = (bf16[8,256,512]{2,1,0:T(8,128)(2,1)S(1)}, bf16[8,256,512]{2,1,0:T(8,128)(2,1)}, u32[]{:S(2)}) copy-start(bf16[8,256,512]{2,1,0:T(8,128)(2,1)} %get-tuple-element.17) | copy-start | bytes 6291460
  119.1 2.3 copy-start.10
  119.1 2.3 copy-start.4
  121.4 2.7 copy-start.13
  158.4 128.1 %copy-start.1 = (bf16[64,2048]{1,0:T(8,128)(2,1)S(1)}, bf16[64,2048]{1,0:T(8,128)(2,1)}, u32[]{:S(2)}) copy-start(bf16[64,2048]{1,0:T(8,128)(2,1)} %param.11) | copy-start | bytes 786436
  158.4 128.1 %copy-start.15 = (f32[2048]{0:T(1024)S(1)}, f32[2048]{0:T(1024)}, u32[]{:S(2)}) copy-start(f32[2048]{0:T(1024)} %param.15) | copy-start | bytes 24580
  284.1 4.2 %copy-start = (bf16[64,2048]{1,0:T(8,128)(2,1)S(1)}, bf16[64,2048]{1,0:T(8,128)(2,1)}, u32[]{:S(2)}) copy-start(bf16[64,2048]{1,0:T(8,128)(2,1)} %param.12) | copy-start | bytes 786436
  284.1 4.2 %copy-start.6 = (bf16[64,2048]{1,0:T(8,128)(2,1)S(1)}, bf16[64,2048]{1,0:T(8,128)(2,1)}, u32[]{:S(2)}) copy-start(bf16[64,2048]{1,0:T(8,128)(2,1)} %get-tuple-element.21) | copy-start | bytes 786436
  284.1 4.2 %copy-start.14 = (f32[2048]{0:T(1024)S(1)}, f32[2048]{0:T(1024)}, u32[]{:S(2)}) copy-start(f32[2048]{0:T(1024)} %param.14) | copy-start | bytes 24580
  284.1 4.4 %copy-start.5 = (bf16[64,2048]{1,0:T(8,128)(2,1)S(1)}, bf16[64,2048]{1,0:T(8,128)(2,1)}, u32[]{:S(2)}) copy-start(bf16[64,2048]{1,0:T(8,128)(2,1)} %grad_ref.1) | copy-start | bytes 786436
  284.1 5.4 %copy-start.7 = (f32[256,1024]{1,0:T(8,128)S(1)}, f32[256,1024]{1,0:T(8,128)}, u32[]{:S(2)}) copy-start(f32[256,1024]{1,0:T(8,128)} %param.19) | copy-start | bytes 3145732
  288.3 2.3 copy-start.12
  289.5 1.6 copy-start.8
  290.6 1.6 copy-start.11
  290.7 1.6 copy-start.9

commit v3 on v2

--- a/solution.py
+++ b/solution.py
@@ -80,10 +80,12 @@
     n_tp,
     late_ref,
     early_ref,
+    gain_ref,
     *refs,
 ):
     w_refs, (late_out, early_out), w_outs = refs[:3], refs[3:5], refs[5:8]
-    tok_send, tok_recv, own_sem, across_send, up_send, down_send, w_recv = refs[8:]
+    gate_out, up_out, hidden_out, normed = refs[8:12]
+    tok_send, tok_recv, own_sem, across_send, up_send, down_send, w_recv = refs[12:]
     at = Place(n_fs, n_tp)
     half = w_outs[0].shape[2]
     kept = pl.ds(pl.multiple_of(at.side * half, half), half)
@@ -133,32 +135,63 @@
             pl.when(high_ok)(down_copy.wait_recv)
         pl.when(high_ok & at.has_down)(down_copy.start)
 
-    for flow in flows:
-        if flow[0] == 0 and flow[2] == 0:
-            run(flow)
+    def run_where(weights, turns, forwarded):
+        for flow in flows:
+            if flow[1] in weights and flow[2] in turns and (flow[0] > 0) == forwarded:
+                run(flow)
+
+    run_where((0, 1), (0,), False)
     for w in range(3):
         own.append(
             pltpu.make_async_copy(w_refs[w].at[:, kept], w_outs[w].at[at.fs], own_sem.at[w])
         )
         own[-1].start()
-    late_out[at.member] = late_ref[...]
-    early_out[at.member] = early_ref[...]
-    for flow in flows:
-        if flow[0] == 0 and flow[2] == 1:
-            run(flow)
-    for offset in range(1, at.group):
-        who = at.member_id((at.member + offset) % at.group)
-        for part, (src, dst) in enumerate(((late_ref, late_out), (early_ref, early_out))):
+    for part, (src, dst) in enumerate(((late_ref, late_out), (early_ref, early_out))):
+        values = src[...].astype(jnp.float32)
+        normed[part] = (values * inverse_rms(values) * gain_ref[...]).astype(jnp.bfloat16)
+        dst[at.member] = normed[part]
+    run_where((0, 1), (1,), False)
+    for part, dst in ((1, early_out), (0, late_out)):
+        for offset in range(1, at.group):
             copy = remote(
-                src, dst.at[at.member], tok_send.at[part, offset], tok_recv.at[part, offset], who
+                normed.at[part],
+                dst.at[at.member],
+                tok_send.at[part, offset],
+                tok_recv.at[part, offset],
+                at.member_id((at.member + offset) % at.group),
             )
             copy.start()
             tokens.append(copy)
-    for flow in flows:
-        if flow[0] > 0:
-            run(flow)
-    for copy in own + tokens:
+    run_where((0,), (0, 1), True)
+    run_where((2,), (0, 1), False)
+    run_where((1,), (0, 1), True)
+    for copy in own:
         copy.wait()
+    for copy in tokens[: at.group - 1]:
+        copy.wait_recv()
+    owners = min(at.group, 4)
+    tile = owners * early_ref.shape[0]
+
+    @pl.loop(0, at.group // owners)
+    def _(i):
+        span = pl.ds(pl.multiple_of(i * tile, tile), tile)
+        rows = early_out[pl.ds(i * owners, owners)].reshape(tile, early_ref.shape[1])
+
+        def product(w):
+            return jnp.dot(
+                rows, w_outs[w][...].reshape(-1, half), preferred_element_type=jnp.float32
+            )
+
+        gate, up = product(0), product(1)
+        gate_out[span] = gate
+        up_out[span] = up
+        hidden_out[span] = (gate * jax.nn.sigmoid(gate) * up).astype(jnp.bfloat16)
+
+    run_where((2,), (0, 1), True)
+    for copy in tokens[at.group - 1 :]:
+        copy.wait_recv()
+    for copy in tokens:
+        copy.wait_send()
     for copy in across:
         copy.wait_send()
     for flow in flows:
@@ -520,21 +553,26 @@
     def shaped(*shape):
         return jax.ShapeDtypeStruct(shape, bf16)
 
-    def normed_of(rows):
-        values = rows.astype(jnp.float32)
-        inverse = inverse_rms(values)
-        return values, inverse, (values * inverse * pre_gain).astype(bf16)
-
-    late_values, _, late_normed = normed_of(late_input)
-    early_values, early_in_inverse, early_own = normed_of(early_input)
+    late_values = late_input.astype(jnp.float32)
+    early_values = early_input.astype(jnp.float32)
+    early_in_inverse = inverse_rms(early_values)
+    preact = jax.ShapeDtypeStruct((group_rows, half), jnp.float32)
     tok_block = shaped(group, tok_rows, model_width)
     w_block = shaped(n_fs, shard_rows, half)
-    late_rows, early_rows, gate_all, up_all, down_all = call(
+    late_rows, early_rows, gate_all, up_all, down_all, early_gate, early_up, early_hidden = call(
         functools.partial(gather_kernel, n_fs, n_tp),
         0,
-        (late_normed, early_own, gate_weight, up_weight, down_weight),
-        [tok_block, tok_block, w_block, w_block, w_block],
+        (
+            late_input,
+            early_input,
+            pre_gain.reshape(1, model_width),
+            gate_weight,
+            up_weight,
+            down_weight,
+        ),
+        [tok_block] * 2 + [w_block] * 3 + [preact, preact, shaped(group_rows, half)],
         [
+            pltpu.VMEM((2, tok_rows, model_width), bf16),
             dma((2, group)),
             dma((2, group)),
             dma((3,)),
@@ -551,15 +589,9 @@
         full.reshape(model_width, half) for full in (gate_all, up_all, down_all)
     )
 
-    def hidden_of(rows):
-        gate_pre = jnp.dot(rows, gate_all, preferred_element_type=jnp.float32)
-        up_pre = jnp.dot(rows, up_all, preferred_element_type=jnp.float32)
-        return gate_pre, up_pre, (jax.nn.silu(gate_pre) * up_pre).astype(bf16)
-
     def by_owner(product):
         return product.astype(bf16).reshape(group, tok_rows, model_width)
 
-    early_gate, early_up, early_hidden = hidden_of(early_rows)
     early_part = by_owner(contract_last(early_hidden, down_all))
     chip_block = pltpu.VMEM((chips, tok_rows, model_width), bf16)
     (cot_rows,) = call(

time: 294 us -> 286 us (0.973)
  matrix products: 8.52 us -> 4.38 us
  other arithmetic: 11.7 us -> 7.56 us
    dot_general x2 -> x0, matrix products: 5.87 us -> none  [the longest x1 3.62 us: hidden_of(): gate_pre = jnp.dot(rows, gate_all, preferred_element_type=jnp.float32)]
where the time goes in v3:
time: 286 us
  Pallas kernels  271 us (95%)
  other arithmetic  7.56 us (3%)
  matrix products  4.38 us (2%)
    pallas_call x3, Pallas kernels, call(): pl.pallas_call(kernel, out_shape=out_shapes, in_specs=[in_vmem] * (len(op...  271 us

profile of v3, /device:TPU:16, one launch (start us, length us, event | category | flops | bytes accessed | tf_op | source)
XLA Modules:
  0.0 285.9 jit_solution(5110987114725073914)
XLA Ops:
  0.6 111.3 %shard_map.146 = (bf16[8,64,2048]{2,1,0:T(8,128)(2,1)}, bf16[8,64,2048]{2,1,0:T(8,128)(2,1)}, bf16[8,256,512]{2,1,0:T(8,128)(2,1)}, bf16[8,256,512]{2,1,0:T(8,12...) custom-call(bf16[64,2048]{1,0:T(8,128)(2,1)} %late_ref.1, ...), custom_call_target="tpu_custom_call" | custom-call | flops 1000000000 | tf_op jit(solution)/shard_map/pallas_call | solution.py:514
  112.0 4.4 %convolution_convert_fusion = bf16[512,2048]{1,0:T(8,128)(2,1)} fusion(bf16[512,512]{1,0:T(8,128)(2,1)} %get-tuple-element.18.refs_1_, bf16[2048,512]{1,0:T(8,128)(2,1)} %bitcast.29), kind=kOutput, calls=%fused_computation | convolution fusion | flops 1074790400 | bytes 4718592 | tf_op jit(solution)/shard_map/dot_general | solution.py:18
  116.4 34.4 %shard_map.147 = bf16[8,64,2048]{2,1,0:T(8,128)(2,1)} custom-call(bf16[8,64,2048]{2,1,0:T(8,128)(2,1)} %bitcast.24, bf16[64,2048]{1,0:T(8,128)(2,1)} %grad_ref.1, f32[1,2048]{1,0:T(1,128)} %bitcast.31), custom_call_target="tpu_custom_call" | custom-call | flops 100000000 | tf_op jit(solution)/shard_map/pallas_call | solution.py:514
  150.7 0.0 copy-start.1
  150.7 0.0 copy-start.10
  150.8 0.0 copy-start.8
  150.8 0.0 copy-start.9
  150.8 125.7 %shard_map.148 = (bf16[2,256,512]{2,1,0:T(8,128)(2,1)}, bf16[2,256,512]{2,1,0:T(8,128)(2,1)}, bf16[2,256,512]{2,1,0:T(8,128)(2,1)}, bf16[64,2048]{1,0:T(8,128)(2,1)}, bf16[64,2048]{1,0:T(8,128)(2,1)}) custom-call(bf16[512,2048]{1,0:T(8,128)(2,1)} %bitcast.23, bf16[512,512]{1,0:T(8,128)(2,1)} %get-tuple-element.18.refs_1_, bf16[512,2048]{1,0:T(8,128)(2,1)} %bitcast.26, ...), custom_call_target="tpu_custom_call" | custom-call | flops 1000000000 | tf_op jit(solution)/shard_map/pallas_call | solution.py:514
  276.5 0.0 copy-start
  276.5 0.0 copy-start.2
  276.5 0.0 copy-start.3
  276.5 1.2 slice_bitcast_fusion.5
  277.7 0.0 copy-done.1
  277.7 0.0 copy-done.10
  277.7 1.3 fusion.4
  279.1 0.0 copy-done.8
  279.1 0.0 copy-done.9
  279.1 0.0 copy-start.6
  279.1 0.0 copy-start.7
  279.1 1.9 fusion.3
  281.0 0.0 copy-done
  281.0 0.0 copy-done.2
  281.0 1.0 fusion.7
  282.0 0.0 copy-done.3
  282.0 0.0 copy-start.4
  282.0 1.1 convert_add_fusion.2
  283.2 0.0 copy-done.6
  283.2 0.0 copy-done.7
  283.2 0.0 copy-start.5
  283.2 0.1 slice_bitcast_fusion.1
  283.2 0.4 copy-done.4
  283.7 1.1 convert_add_fusion
  284.8 0.0 copy-done.5
  284.8 1.1 convert_add_fusion.1
  (3 shorter events, 0.0 us)
Async XLA Ops:
  150.7 127.0 %copy-start.1 = (bf16[64,2048]{1,0:T(8,128)(2,1)S(1)}, bf16[64,2048]{1,0:T(8,128)(2,1)}, u32[]{:S(2)}) copy-start(bf16[64,2048]{1,0:T(8,128)(2,1)} %early_ref.1) | copy-start | bytes 786436
  150.7 127.0 %copy-start.10 = (f32[2048]{0:T(1024)S(1)}, f32[2048]{0:T(1024)}, u32[]{:S(2)}) copy-start(f32[2048]{0:T(1024)} %param.14) | copy-start | bytes 24580
  150.8 128.3 %copy-start.8 = (bf16[64,2048]{1,0:T(8,128)(2,1)S(1)}, bf16[64,2048]{1,0:T(8,128)(2,1)}, u32[]{:S(2)}) copy-start(bf16[64,2048]{1,0:T(8,128)(2,1)} %late_ref.1) | copy-start | bytes 786436
  150.8 128.3 %copy-start.9 = (f32[2048]{0:T(1024)S(1)}, f32[2048]{0:T(1024)}, u32[]{:S(2)}) copy-start(f32[2048]{0:T(1024)} %param.15) | copy-start | bytes 24580
  276.5 4.6 %copy-start = (bf16[64,2048]{1,0:T(8,128)(2,1)S(1)}, bf16[64,2048]{1,0:T(8,128)(2,1)}, u32[]{:S(2)}) copy-start(bf16[64,2048]{1,0:T(8,128)(2,1)} %grad_ref.1) | copy-start | bytes 786436
  276.5 4.5 %copy-start.2 = (bf16[64,2048]{1,0:T(8,128)(2,1)S(1)}, bf16[64,2048]{1,0:T(8,128)(2,1)}, u32[]{:S(2)}) copy-start(bf16[64,2048]{1,0:T(8,128)(2,1)} %get-tuple-element.27) | copy-start | bytes 786436
  276.5 5.5 %copy-start.3 = (f32[256,1024]{1,0:T(8,128)S(1)}, f32[256,1024]{1,0:T(8,128)}, u32[]{:S(2)}) copy-start(f32[256,1024]{1,0:T(8,128)} %param.19) | copy-start | bytes 3145732
  279.1 4.0 %copy-start.6 = (bf16[2,256,512]{2,1,0:T(8,128)(2,1)S(1)}, bf16[2,256,512]{2,1,0:T(8,128)(2,1)}, u32[]{:S(2)}) copy-start(bf16[2,256,512]{2,1,0:T(8,128)(2,1)} %get-tuple-element.29) | copy-start | bytes 1572868
  279.1 4.0 %copy-start.7 = (bf16[2,256,512]{2,1,0:T(8,128)(2,1)S(1)}, bf16[2,256,512]{2,1,0:T(8,128)(2,1)}, u32[]{:S(2)}) copy-start(bf16[2,256,512]{2,1,0:T(8,128)(2,1)} %get-tuple-element.30) | copy-start | bytes 1572868
  282.0 1.6 copy-start.4
  283.2 1.6 copy-start.5
